TPU v7x, 32 devices: a whole 2x2x4 slice. The times are simulated.
32 devices in a mesh: fs: 4 (over z), tp: 8 (over y, x, core).
Axes of the slice: x: 2, y: 2, z: 4, core: 2. Of those that a mesh axis runs over, the one named last changes fastest.
Arguments:
- saved_input: bfloat16 [4096, 2304], P('fs', 'tp'), may hold values from -6 to 6
- cot_forget: bfloat16 [4096, 2304], P('fs', 'tp'), may hold values from -0.09375 to 0.09375
- cot_value: bfloat16 [4096, 2304], P('fs', 'tp'), may hold values from -0.09375 to 0.09375
- basis_forget: bfloat16 [2304, 288], replicated, may hold values from -2 to 2
- basis_value: bfloat16 [2304, 288], replicated, may hold values from -2 to 2
- first_forget: float32 [288, 2304], P('fs', 'tp'), may hold values from -180 to 180
- first_value: float32 [288, 2304], P('fs', 'tp'), may hold values from -180 to 180
- second_forget: float32 [288, 2304], P('fs', 'tp'), may hold values from 0.1 to 1
- second_value: float32 [288, 2304], P('fs', 'tp'), may hold values from 0.1 to 1
- weight_forget: float32 [2304, 2304], P('fs', 'tp'), may hold values from -0.125 to 0.125
- weight_value: float32 [2304, 2304], P('fs', 'tp'), may hold values from -0.125 to 0.125
Outputs:
- new_first_forget: float32 [288, 2304], P('fs', 'tp')
- new_second_forget: float32 [288, 2304], P('fs', 'tp')
- step_forget: float32 [2304, 2304], P('fs', 'tp')
- new_weight_forget: float32 [2304, 2304], P('fs', 'tp')
- copy_forget: bfloat16 [2304, 2304], P(None, 'tp')
- new_first_value: float32 [288, 2304], P('fs', 'tp')
- new_second_value: float32 [288, 2304], P('fs', 'tp')
- step_value: float32 [2304, 2304], P('fs', 'tp')
- new_weight_value: float32 [2304, 2304], P('fs', 'tp')
- copy_value: bfloat16 [2304, 2304], P(None, 'tp')
All inputs are finite; a program needn't handle non-finite values.
Results may differ from a plain program's by a relative error of at most 0.0042.
Values may be sent and summed in bfloat16 or wider, within the bound.
A program may use at most 64 MiB of HBM per device.

v0:
```python
import jax
import jax.numpy as jnp
from jax import lax
from jax.sharding import PartitionSpec as P

D = 2304


beta_one = 0.8
beta_two = 0.9
rate = 0.02
epsilon = 1e-06


def contract(left_part, right_part):
    return lax.dot_general(
        left_part,
        right_part,
        (((0,), (0,)), ((), ())),
        precision=lax.Precision.HIGHEST,
        preferred_element_type=jnp.float32,
    )


def moments(projected, first, second):
    new_first = beta_one * first + (1.0 - beta_one) * projected
    new_second = beta_two * second + (1.0 - beta_two) * projected * projected
    direction = (new_first / jnp.sqrt(new_second)).astype(jnp.bfloat16)
    return (new_first, new_second, direction)


def body(
    saved_input,
    cot_forget,
    cot_value,
    basis_forget,
    basis_value,
    first_forget,
    first_value,
    second_forget,
    second_value,
    weight_forget,
    weight_value,
):
    col_width = cot_forget.shape[1]
    own_rows = weight_forget.shape[0]
    col_first = lax.axis_index("tp") * col_width
    row_start = lax.axis_index("fs") * own_rows
    rows_forget = lax.dynamic_slice_in_dim(basis_forget, row_start, own_rows, 0)
    rows_value = lax.dynamic_slice_in_dim(basis_value, row_start, own_rows, 0)
    both_cots = jnp.concatenate([cot_forget, cot_value], axis=1)
    cols_forget = lax.dynamic_slice_in_dim(basis_forget, col_first, col_width, 0)
    cols_value = lax.dynamic_slice_in_dim(basis_value, col_first, col_width, 0)
    partial_forget = jnp.dot(saved_input, cols_forget, preferred_element_type=jnp.float32)
    partial_value = jnp.dot(saved_input, cols_value, preferred_element_type=jnp.float32)
    summed_forget, summed_value = lax.psum((partial_forget, partial_value), "tp")
    cots_wide = both_cots.astype(jnp.float32)
    projected = lax.psum_scatter(
        jnp.concatenate(
            [
                contract(summed_forget, cots_wide[:, :col_width]),
                contract(summed_value, cots_wide[:, col_width:]),
            ],
            axis=1,
        ),
        "fs",
        scatter_dimension=0,
        tiled=True,
    )
    new_first_forget, new_second_forget, direction_forget = moments(
        projected[:, :col_width], first_forget, second_forget
    )
    new_first_value, new_second_value, direction_value = moments(
        projected[:, col_width:], first_value, second_value
    )
    update_forget = jnp.dot(
        rows_forget,
        lax.all_gather(direction_forget, "fs", axis=0, tiled=True),
        preferred_element_type=jnp.float32,
    )
    update_value = jnp.dot(
        rows_value,
        lax.all_gather(direction_value, "fs", axis=0, tiled=True),
        preferred_element_type=jnp.float32,
    )
    square_forget, square_value = lax.psum(
        (jnp.sum(update_forget * update_forget), jnp.sum(update_value * update_value)), ("fs", "tp")
    )
    entries = float(D * D)
    step_forget = update_forget / jnp.sqrt(square_forget / entries + epsilon)
    step_value = update_value / jnp.sqrt(square_value / entries + epsilon)
    new_weight_forget = weight_forget - rate * step_forget
    new_weight_value = weight_value - rate * step_value
    copy_forget, copy_value = (
        lax.all_gather(new_weight_forget.astype(jnp.bfloat16), "fs", axis=0, tiled=True),
        lax.all_gather(new_weight_value.astype(jnp.bfloat16), "fs", axis=0, tiled=True),
    )
    return (
        new_first_forget,
        new_second_forget,
        step_forget,
        new_weight_forget,
        copy_forget,
        new_first_value,
        new_second_value,
        step_value,
        new_weight_value,
        copy_value,
    )


def solution(mesh):
    in_specs = (
        P("fs", "tp"),
        P("fs", "tp"),
        P("fs", "tp"),
        P(),
        P(),
        P("fs", "tp"),
        P("fs", "tp"),
        P("fs", "tp"),
        P("fs", "tp"),
        P("fs", "tp"),
        P("fs", "tp"),
    )
    out_specs = (
        P("fs", "tp"),
        P("fs", "tp"),
        P("fs", "tp"),
        P("fs", "tp"),
        P(None, "tp"),
        P("fs", "tp"),
        P("fs", "tp"),
        P("fs", "tp"),
        P("fs", "tp"),
        P(None, "tp"),
    )
    return jax.shard_map(body, mesh=mesh, in_specs=in_specs, out_specs=out_specs, check_vma=False)
```

profile of v0, /device:TPU:0, one launch (start us, length us, event | category | flops | bytes accessed | tf_op | source)
XLA Modules:
  0.0 281.1 jit_solution(6766802220933161074)
XLA Ops:
  7.3 2.8 %convolution_bitcast_fusion = f32[1024,288]{0,1:T(8,128)} fusion(bf16[1024,288]{0,1:T(8,128)(2,1)} %param.11, bf16[2304,288]{0,1:T(8,128)(2,1)} %param.15, s32[]{:T(128)S(6)} %select_n.8), kind=kOutput, calls=%fused_computation | convolution fusion | flops 169869312 | bytes 1990660 | tf_op jit(solution)/shard_map/dot_general | solution.py:55
  10.1 1.5 convolution_bitcast_fusion.1
  11.6 0.0 all-reduce.6.cloned.1.call-start
  11.7 66.5 %all-reduce.8.cloned.1.call-done = (f32[1024,288]{0,1:T(8,128)}, f32[1024,288]{0,1:T(8,128)}) async-done(((f32[1024,288]{0,1:T(8,128)}, f32[1024,288]{0,1:T(8,128)}), (f32[1024,288]{0,1:T(8,128)}, f32[1024,288]{0,1:T(8,128)})) %all-reduce.8.cloned.1.call-update) | async-done | bytes 2359312 | tf_op jit(solution)/shard_map/psum | solution.py:56
  78.2 2.4 fusion.15
  80.7 1.1 fusion.14
  81.8 1.0 pad_maximum_fusion
  82.9 0.0 all-gather.5.cloned.1.call-start
  83.0 0.6 dynamic-slice
  84.2 40.8 %all-reduce.6.cloned.1.call-done = f32[288,576]{1,0:T(8,128)} async-done(((f32[288,576]{1,0:T(8,128)}), f32[288,576]{1,0:T(8,128)}) %all-reduce.6.cloned.1.call-update) | async-done | bytes 663568
  125.0 1.8 multiply_convert_fusion
  126.9 14.1 %all_gather.14 = bf16[288,288]{1,0:T(8,128)(2,1)S(1)} all-gather(bf16[72,288]{1,0:T(8,128)(2,1)S(1)} %get-tuple-element.20), channel_id=1, replica_groups=mesh['fs'=4,'tp'=8] {'fs'}, dimensions={0}, use_global_device_ids=true | all-gather | bytes 207360 | tf_op jit(solution)/shard_map/all_gather | solution.py:83
  141.0 13.7 %all_gather.12 = bf16[288,288]{1,0:T(8,128)(2,1)S(1)} all-gather(bf16[72,288]{1,0:T(8,128)(2,1)S(1)} %get-tuple-element.26), channel_id=1, replica_groups=mesh['fs'=4,'tp'=8] {'fs'}, dimensions={0}, use_global_device_ids=true | all-gather | bytes 207360 | tf_op jit(solution)/shard_map/all_gather | solution.py:78
  154.7 1.2 multiply_reduce_fusion.1
  155.9 2.2 multiply_reduce_fusion
  158.1 39.0 %all-reduce.1 = (f32[]{:T(128)}, f32[]{:T(128)}) all-reduce(f32[]{:T(128)} %get-tuple-element.29, f32[]{:T(128)} %get-tuple-element.31), channel_id=1, replica_groups=mesh['fs'=4,'tp'=8] {'fs','tp'}, use_global_device_ids=true, to_apply=%region_4.0 | all-reduce | flops 2 | bytes 16 | tf_op jit(solution)/shard_map/psum | solution.py:86
  197.7 1.4 convert_bitcast_fusion.1
  199.9 2.5 convert_bitcast_fusion
  202.3 32.4 %all-gather.5.cloned.1.call-done = bf16[4,576,288]{1,2,0:T(8,128)(2,1)} async-done(((bf16[1,576,288]{1,2,0:T(8,128)(2,1)}), bf16[4,576,288]{1,2,0:T(8,128)(2,1)}) %all-gather.5.cloned.1.call-update) | async-done | bytes 1327120 | tf_op jit(solution)/shard_map/all_gather | solution.py:95
  234.7 2.1 copy.23
  236.9 2.0 reshape.21
  238.9 31.6 %all-gather.7.cloned.1.call-done = bf16[4,576,288]{1,2,0:T(8,128)(2,1)} async-done(((bf16[1,576,288]{1,2,0:T(8,128)(2,1)}), bf16[4,576,288]{1,2,0:T(8,128)(2,1)}) %all-gather.7.cloned.1.call-update) | async-done | bytes 1327120 | tf_op jit(solution)/shard_map/all_gather | solution.py:96
  270.5 2.1 copy.24
  272.6 2.0 reshape.23
  (28 shorter events, 0.2 us)
Async XLA Ops:
  7.2 2.9 %copy-start = (bf16[2304,288]{0,1:T(8,128)(2,1)S(1)}, bf16[2304,288]{0,1:T(8,128)(2,1)}, u32[]{:S(2)}) copy-start(bf16[2304,288]{0,1:T(8,128)(2,1)} %param.14) | copy-start | bytes 3981316
  7.2 2.9 %copy-start.1 = (bf16[1024,288]{0,1:T(8,128)(2,1)S(1)}, bf16[1024,288]{0,1:T(8,128)(2,1)}, u32[]{:S(2)}) copy-start(bf16[1024,288]{0,1:T(8,128)(2,1)} %param.11) | copy-start | bytes 1769476
  7.2 71.0 %all-reduce.8.cloned.1.call-start = ((), (), s32[]{:S(2)}) async-start(), calls=%async_computation.3 | async-start | bytes 4718592 | tf_op jit(solution)/shard_map/psum | solution.py:56
  11.6 66.6 %copy-start.4 = (bf16[1024,288]{0,1:T(8,128)(2,1)S(1)}, bf16[1024,288]{0,1:T(8,128)(2,1)}, u32[]{:S(2)}) copy-start(bf16[1024,288]{0,1:T(8,128)(2,1)} %param.13) | copy-start | bytes 1769476
  11.6 69.1 %copy-start.5 = (bf16[1024,288]{0,1:T(8,128)(2,1)S(1)}, bf16[1024,288]{0,1:T(8,128)(2,1)}, u32[]{:S(2)}) copy-start(bf16[1024,288]{0,1:T(8,128)(2,1)} %param.12) | copy-start | bytes 1769476
  11.6 113.4 %all-reduce.6.cloned.1.call-start = ((), (), s32[]{:S(2)}) async-start(), calls=%async_computation.2 | async-start | bytes 1474560
  78.2 2.5 copy-start.2
  81.8 1.2 copy-start.10
  81.8 43.2 %copy-start.6 = (f32[72,288]{1,0:T(8,128)S(1)}, f32[72,288]{1,0:T(8,128)}, u32[]{:S(2)}) copy-start(f32[72,288]{1,0:T(8,128)} %param.19) | copy-start | bytes 248836
  81.8 43.2 %copy-start.7 = (f32[72,288]{1,0:T(8,128)S(1)}, f32[72,288]{1,0:T(8,128)}, u32[]{:S(2)}) copy-start(f32[72,288]{1,0:T(8,128)} %param.17) | copy-start | bytes 248836
  81.8 43.2 %copy-start.8 = (f32[72,288]{1,0:T(8,128)S(1)}, f32[72,288]{1,0:T(8,128)}, u32[]{:S(2)}) copy-start(f32[72,288]{1,0:T(8,128)} %param.18) | copy-start | bytes 248836
  81.8 43.2 %copy-start.9 = (f32[72,288]{1,0:T(8,128)S(1)}, f32[72,288]{1,0:T(8,128)}, u32[]{:S(2)}) copy-start(f32[72,288]{1,0:T(8,128)} %param.16) | copy-start | bytes 248836
  82.9 151.8 %all-gather.5.cloned.1.call-start = ((), (), s32[]{:S(2)}) async-start(), calls=%async_computation | async-start | bytes 1843200 | tf_op jit(solution)/shard_map/all_gather | solution.py:95
  154.7 43.1 %copy-start.3 = (f32[576,288]{0,1:T(8,128)S(1)}, f32[576,288]{0,1:T(8,128)}, u32[]{:S(2)}) copy-start(f32[576,288]{0,1:T(8,128)} %param.20) | copy-start | bytes 1990660
  199.1 71.4 %all-gather.7.cloned.1.call-start = ((), (), s32[]{:S(2)}) async-start(), calls=%async_computation.1 | async-start | bytes 1843200 | tf_op jit(solution)/shard_map/all_gather | solution.py:96
Sparse Core Ops, SparseCore 0:
  12.5 65.7 all-reduce.7
  83.0 41.9 all-reduce.5
  199.2 35.4 all-gather.4
  236.1 34.2 all-gather.6
where the time goes:
time: 282 us; the launch traced here: 281 us
  waiting for transfers between devices  171 us (61%)
  blocking collectives  66.8 us (24%)
  between operations  16 us (6%)
  matrix products  11.2 us (4%)
  local copies, waits for them, and re-layouts  8.9 us (3%)
  other arithmetic  6.67 us (2%)
    psum x1, waiting for transfers between devices, body(): lax.psum((partial_forget, partial_value), 'tp')  66.5 us
    unnamed x5, waiting for transfers between devices  40.9 us
    psum x1, blocking collectives, body(): lax.psum((jnp.sum(update_forget * update_forget), jnp.sum(update_value *...  39 us
    all_gather x1, waiting for transfers between devices, body(): lax.all_gather(new_weight_forget.astype(jnp.bfloat16), 'fs', axis=0, tile...  32.4 us
    all_gather x1, waiting for transfers between devices, body(): lax.all_gather(new_weight_value.astype(jnp.bfloat16), 'fs', axis=0, tiled...  31.6 us
    all_gather x1, blocking collectives, body(): lax.all_gather(direction_value, 'fs', axis=0, tiled=True)  14.1 us
    all_gather x1, blocking collectives, body(): lax.all_gather(direction_forget, 'fs', axis=0, tiled=True)  13.7 us
  transfers between devices with their start and end apart: 4, of which 4 were waited for; matrix products, arithmetic and copies ran while one was open for 3% of the time, Pallas kernels for 0%

commit v1 on v0

--- a/solution.py
+++ b/solution.py
@@ -1,10 +1,14 @@
+import functools
+
 import jax
 import jax.numpy as jnp
 from jax import lax
+from jax.experimental import pallas as pl
+from jax.experimental.pallas import tpu as pltpu
 from jax.sharding import PartitionSpec as P
 
-D = 2304
-
+MESH = pl.DeviceIdType.MESH
+LANES = 128
 
 beta_one = 0.8
 beta_two = 0.9
@@ -86,7 +90,7 @@
     square_forget, square_value = lax.psum(
         (jnp.sum(update_forget * update_forget), jnp.sum(update_value * update_value)), ("fs", "tp")
     )
-    entries = float(D * D)
+    entries = float(basis_forget.shape[0] * weight_forget.shape[1] * lax.axis_size("tp"))
     step_forget = update_forget / jnp.sqrt(square_forget / entries + epsilon)
     step_value = update_value / jnp.sqrt(square_value / entries + epsilon)
     new_weight_forget = weight_forget - rate * step_forget
@@ -109,30 +113,378 @@
     )
 
 
+def pack(weights, odd, half):
+    deep = weights[0].shape[0] // 2
+    cols = weights[0].shape[1]
+    side = LANES // 2
+    whole = cols - side
+    tiles = []
+    rests = []
+    for weight in weights:
+        rows = weight[deep * half : deep * (half + 1)]
+        kept = jnp.where(odd, rows[:, side:], rows[:, :whole])
+        tiles += [kept[:, at : at + LANES] for at in range(0, whole, LANES)]
+        rests.append(jnp.where(odd, rows[:, :side], rows[:, whole:]))
+    rest = jnp.where(
+        odd,
+        jnp.concatenate([rests[1], rests[0]], axis=1),
+        jnp.concatenate(rests, axis=1),
+    )
+    return jnp.stack(tiles + [rest]).astype(jnp.bfloat16)
+
+
+def new_moments(projected, first, second):
+    new_first = beta_one * first + (1.0 - beta_one) * projected
+    new_second = beta_two * second + (1.0 - beta_two) * projected * projected
+    return new_first, new_second
+
+
+def contract_tokens(left, right):
+    return lax.dot_general(
+        left, right, (((1,), (1,)), ((), ())), preferred_element_type=jnp.float32
+    )
+
+
+def exchange(
+    F, T,
+    s_hbm, cf_hbm, cv_hbm, bf_hbm, bv_hbm, ff_hbm, fv_hbm, sf_hbm, sv_hbm, wf_hbm, wv_hbm,
+    pr_out, d_out, ss_out, wg_out,
+    s, c, b, fm, sm, w, sg, z, zg, psend, prx, pr, dg, d, ss, wg,
+    in_sem, sg_own, sg_send, sg_recv, z_send, z_recv, zf_send, zf_recv,
+    p_send, p_recv, d_send, d_recv, n_send, n_recv, w_send, w_recv, wl_send, wl_recv, out_sem, wo_sem,
+):
+    f = lax.axis_index("fs")
+    t = lax.axis_index("tp")
+    ranks = psend.shape[1] // 2
+    block = zg.shape[3]
+    right = lax.rem(f + 1, F)
+    left = lax.rem(f + F - 1, F)
+    far = lax.rem(f + 2, F)
+    pair = t + 1 - 2 * lax.rem(t, 2)
+
+    def tp_at(k):
+        return lax.rem(t + k + T, T)
+
+    def fs_at(k):
+        return lax.rem(f + k + F, F)
+
+    def tokens(k):
+        return pl.ds(pl.multiple_of(k * block, block), block)
+
+    def fetch(src, dst, sem):
+        copy = pltpu.make_async_copy(src, dst, sem)
+        copy.start()
+        return copy
+
+    def push(src, dst, send, recv, where):
+        return pltpu.make_async_remote_copy(
+            src_ref=src, dst_ref=dst, send_sem=send, recv_sem=recv,
+            device_id=where, device_id_type=MESH,
+        )
+
+    load_w = [fetch(wf_hbm, w.at[0], in_sem.at[0]), fetch(wv_hbm, w.at[1], in_sem.at[1])]
+    load_s = fetch(s_hbm, s, in_sem.at[2])
+    load_own = fetch(s_hbm.at[:, tokens(t)], sg.at[t], sg_own)
+    load_b = [fetch(bf_hbm, b.at[0], in_sem.at[3]), fetch(bv_hbm, b.at[1], in_sem.at[4])]
+    load_c = [fetch(cf_hbm, c.at[0], in_sem.at[5]), fetch(cv_hbm, c.at[1], in_sem.at[6])]
+    load_m = [
+        fetch(ff_hbm, fm.at[0], in_sem.at[7]), fetch(fv_hbm, fm.at[1], in_sem.at[8]),
+        fetch(sf_hbm, sm.at[0], in_sem.at[9]), fetch(sv_hbm, sm.at[1], in_sem.at[10]),
+    ]
+
+    barrier = pltpu.get_barrier_semaphore()
+    for k in range(1, T):
+        pl.semaphore_signal(barrier, inc=1, device_id={"tp": tp_at(k)}, device_id_type=MESH)
+    for k in range(1, F):
+        pl.semaphore_signal(barrier, inc=1, device_id={"fs": fs_at(k)}, device_id_type=MESH)
+    for p in range(2):
+        load_w[p].wait()
+    both = [w[0], w[1]]
+    for half in range(2):
+        wg[f, half] = pack(both, lax.rem(f, 2) == 1, half)
+    load_s.wait()
+    pl.semaphore_wait(barrier, T + F - 2)
+
+    sends = []
+    for k in range(1, T):
+        copy = push(s.at[:, tokens(tp_at(k))], sg.at[t], sg_send.at[k], sg_recv.at[k], {"tp": tp_at(k)})
+        copy.start()
+        sends.append(copy)
+    own_right = [push(wg.at[f, p], wg.at[f, p], w_send.at[p], w_recv.at[p], {"fs": right}) for p in range(2)]
+    own_left = [push(wg.at[f, p], wg.at[f, p], wl_send.at[p], wl_recv.at[p], {"fs": left}) for p in range(2)]
+    own_right[0].start()
+    own_left[1].start()
+    own_right[1].start()
+    own_left[0].start()
+    sends += own_right + own_left
+
+    load_own.wait()
+    for copy in load_b:
+        copy.wait()
+    for k in range(1, T):
+        source = tp_at(-k)
+        push(s.at[:, tokens(t)], sg.at[source], sg_send.at[k], sg_recv.at[k], {"tp": source}).wait_recv()
+    inputs = sg[...].reshape(b.shape[2], block)
+    for p in range(2):
+        z[p] = jnp.dot(b[p], inputs, preferred_element_type=jnp.float32).astype(jnp.bfloat16)
+
+    chips = T // 2
+    to_pair = push(z, zg.at[t], zf_send.at[0], zf_recv.at[0], {"tp": pair})
+    for k in range(1, chips):
+        copy = push(z, zg.at[t], z_send.at[k], z_recv.at[k], {"tp": tp_at(2 * k)})
+        copy.start()
+        sends.append(copy)
+    to_pair.start()
+    sends.append(to_pair)
+
+    for copy in load_c:
+        copy.wait()
+    partial = [contract_tokens(z[p], c[p, :, tokens(t)]) for p in range(2)]
+
+    def add(partial, source):
+        return [
+            partial[p] + contract_tokens(zg[source, p], c[p, :, tokens(source)])
+            for p in range(2)
+        ]
+
+    push(z, zg.at[pair], zf_send.at[0], zf_recv.at[0], {"tp": pair}).wait_recv()
+    partial = add(partial, pair)
+    for k in range(1, chips):
+        source = tp_at(-2 * k)
+        push(z, zg.at[source], z_send.at[k], z_recv.at[k], {"tp": source}).wait_recv()
+        copy = push(zg.at[source], zg.at[source], zf_send.at[k], zf_recv.at[k], {"tp": pair})
+        copy.start()
+        sends.append(copy)
+        partial = add(partial, source)
+    for k in range(1, chips):
+        source = lax.rem(pair - 2 * k + T, T)
+        push(z, zg.at[source], zf_send.at[k], zf_recv.at[k], {"tp": pair}).wait_recv()
+        partial = add(partial, source)
+
+    for q in range(F):
+        rows = jnp.concatenate([part[q * ranks : (q + 1) * ranks] for part in partial], axis=0)
+        psend[q] = rows.astype(jnp.bfloat16)
+        own = jnp.where(f == q, rows, 0.0)
+        total = own if q == 0 else total + own
+    for k in (1, F - 1, *range(2, F - 1)):
+        copy = push(psend.at[fs_at(k)], prx.at[f], p_send.at[k], p_recv.at[k], {"fs": fs_at(k)})
+        copy.start()
+        sends.append(copy)
+
+    push(wg.at[f, 0], wg.at[left, 0], w_send.at[0], w_recv.at[0], {"fs": left}).wait_recv()
+    on_right = push(wg.at[left, 0], wg.at[left, 0], w_send.at[2], w_recv.at[2], {"fs": right})
+    on_right.start()
+    push(wg.at[f, 1], wg.at[right, 1], wl_send.at[1], wl_recv.at[1], {"fs": right}).wait_recv()
+    on_left = push(wg.at[right, 1], wg.at[right, 1], wl_send.at[2], wl_recv.at[2], {"fs": left})
+    on_left.start()
+    sends += [on_right, on_left]
+
+    for copy in load_m:
+        copy.wait()
+    for k in (1, F - 1, *range(2, F - 1)):
+        push(psend.at[f], prx.at[fs_at(-k)], p_send.at[k], p_recv.at[k], {"fs": fs_at(-k)}).wait_recv()
+    for k in range(1, F):
+        total = total + prx[fs_at(-k)].astype(jnp.float32)
+    pr[...] = total
+    new_first, new_second = new_moments(total, fm[...].reshape(total.shape), sm[...].reshape(total.shape))
+    dg[f] = (new_first / jnp.sqrt(new_second)).astype(jnp.bfloat16)
+    outs = [fetch(pr, pr_out, out_sem.at[0])]
+    for k in (1, F - 1, *range(2, F - 1)):
+        copy = push(dg.at[f], dg.at[f], d_send.at[k], d_recv.at[k], {"fs": fs_at(k)})
+        copy.start()
+        sends.append(copy)
+    for k in (1, F - 1, *range(2, F - 1)):
+        push(dg.at[f], dg.at[fs_at(-k)], d_send.at[k], d_recv.at[k], {"fs": fs_at(-k)}).wait_recv()
+    gathered = dg[...].astype(jnp.float32)
+    for p in range(2):
+        d[p] = jnp.concatenate(
+            [gathered[q, p * ranks : (p + 1) * ranks] for q in range(F)], axis=0
+        ).T.astype(jnp.bfloat16)
+    outs.append(fetch(d, d_out, out_sem.at[1]))
+
+    for p in range(2):
+        squares = jnp.zeros((d.shape[1], LANES), jnp.float32)
+        update = jnp.dot(d[p], b[p], preferred_element_type=jnp.float32)
+        for at in range(0, update.shape[1], LANES):
+            part = update[:, at : at + LANES]
+            squares = squares + part * part
+        ss[t, p] = jnp.full((8, LANES), jnp.sum(squares), jnp.float32)
+    for k in range(1, T):
+        copy = push(ss.at[t], ss.at[t], n_send.at[k], n_recv.at[k], {"tp": tp_at(k)})
+        copy.start()
+        sends.append(copy)
+    for k in range(1, T):
+        push(ss.at[t], ss.at[tp_at(-k)], n_send.at[k], n_recv.at[k], {"tp": tp_at(-k)}).wait_recv()
+    outs.append(fetch(ss, ss_out, out_sem.at[2]))
+
+    outs.append(fetch(wg.at[f], wg_out.at[f], wo_sem.at[0]))
+    push(wg.at[f, 1], wg.at[left, 1], w_send.at[1], w_recv.at[1], {"fs": left}).wait_recv()
+    outs.append(fetch(wg.at[left], wg_out.at[left], wo_sem.at[1]))
+    push(wg.at[f, 0], wg.at[right, 0], wl_send.at[0], wl_recv.at[0], {"fs": right}).wait_recv()
+    outs.append(fetch(wg.at[right], wg_out.at[right], wo_sem.at[2]))
+    push(wg.at[left, 0], wg.at[far, 0], w_send.at[2], w_recv.at[2], {"fs": left}).wait_recv()
+    push(wg.at[right, 1], wg.at[far, 1], wl_send.at[2], wl_recv.at[2], {"fs": right}).wait_recv()
+    outs.append(fetch(wg.at[far], wg_out.at[far], wo_sem.at[3]))
+    for copy in outs:
+        copy.wait()
+    for copy in sends:
+        copy.wait_send()
+
+
+def finish(
+    F, entries,
+    at_ref, pr, d, ss, wg, bf, bv, wf, wv, ff, fv, sf, sv,
+    nff, nsf, stf, nwf, cof, nfv, nsv, stv, nwv, cov,
+):
+    f = at_ref[0]
+    low = lax.broadcasted_iota(jnp.int32, (wg.shape[3], LANES), 1) < LANES // 2
+    ranks = ff.shape[0]
+    tiles = wg.shape[2] // 2
+    cols = wf.shape[1]
+    for p, (basis, weight, first, second, nf, ns, step, nw, copy) in enumerate(
+        ((bf, wf, ff, sf, nff, nsf, stf, nwf, cof), (bv, wv, fv, sv, nfv, nsv, stv, nwv, cov))
+    ):
+        @pl.when(pl.program_id(0) == 0)
+        def _():
+            nf[...], ns[...] = new_moments(pr[p * ranks : (p + 1) * ranks], first[...], second[...])
+
+        square = ss[0, p, 0:1, 0:1]
+        for q in range(1, ss.shape[0]):
+            square = square + ss[q, p, 0:1, 0:1]
+        scale = 1.0 / jnp.sqrt(square / entries + epsilon)
+        steps = jnp.dot(d[p], basis[...], preferred_element_type=jnp.float32) * scale
+        own = steps[:, :cols]
+        for q in range(1, F):
+            own = jnp.where(f == q, steps[:, q * cols : (q + 1) * cols], own)
+        step[...] = own
+        nw[...] = weight[...] - rate * own
+        parts = []
+        for q in range(0, F, 2):
+            parts += [wg[q, 0, p * tiles + i].astype(jnp.float32) for i in range(tiles)]
+            even = wg[q, 0, 2 * tiles].astype(jnp.float32)
+            odd = wg[q + 1, 0, 2 * tiles].astype(jnp.float32)
+            if p == 0:
+                parts.append(jnp.where(low, even, odd))
+            else:
+                parts.append(pltpu.roll(jnp.where(low, odd, even), LANES // 2, 1))
+            parts += [wg[q + 1, 0, p * tiles + i].astype(jnp.float32) for i in range(tiles)]
+        for i, part in enumerate(parts):
+            at = i * LANES
+            copy[:, at : at + LANES] = (part - rate * steps[:, at : at + LANES]).astype(jnp.bfloat16)
+
+
+def kernel_body(
+    F, T,
+    saved_input, cot_forget, cot_value, basis_forget, basis_value,
+    first_forget, first_value, second_forget, second_value, weight_forget, weight_value,
+):
+    tokens, cols = saved_input.shape
+    width, rank = basis_forget.shape
+    ranks = first_forget.shape[0]
+    rows = weight_forget.shape[0]
+    block = tokens // T
+    tiles = 2 * (rows // LANES) + 1
+    half = cols // 2
+    f32, bf16 = jnp.float32, jnp.bfloat16
+    DMA = pltpu.SemaphoreType.DMA
+    VMEM = pltpu.VMEM
+    anywhere = pl.BlockSpec(memory_space=pl.ANY)
+    in_hbm = pl.BlockSpec(memory_space=pltpu.HBM)
+    bases = (basis_forget.T, basis_value.T)
+    weights = (weight_forget.T, weight_value.T)
+    moments_in = (first_forget, first_value, second_forget, second_value)
+
+    projected, direction, squares, gathered = pl.pallas_call(
+        functools.partial(exchange, F, T),
+        out_shape=(
+            jax.ShapeDtypeStruct((2 * ranks, cols), f32),
+            jax.ShapeDtypeStruct((2, cols, rank), bf16),
+            jax.ShapeDtypeStruct((T, 2, 8, LANES), f32),
+            jax.ShapeDtypeStruct((F, 2, tiles, half, LANES), bf16),
+        ),
+        in_specs=[in_hbm] * 11,
+        out_specs=(anywhere,) * 4,
+        scratch_shapes=[
+            VMEM((cols, tokens), bf16),
+            VMEM((2, cols, tokens), bf16),
+            VMEM((2, rank, width), bf16),
+            VMEM((2, ranks, cols), f32),
+            VMEM((2, ranks, cols), f32),
+            VMEM((2, cols, rows), f32),
+            VMEM((T, cols, block), bf16),
+            VMEM((2, rank, block), bf16),
+            VMEM((T, 2, rank, block), bf16),
+            VMEM((F, 2 * ranks, cols), bf16),
+            VMEM((F, 2 * ranks, cols), bf16),
+            VMEM((2 * ranks, cols), f32),
+            VMEM((F, 2 * ranks, cols), bf16),
+            VMEM((2, cols, rank), bf16),
+            VMEM((T, 2, 8, LANES), f32),
+            VMEM((F, 2, tiles, half, LANES), bf16),
+            DMA((11,)), DMA, DMA((T,)), DMA((T,)), DMA((T,)), DMA((T,)), DMA((T,)), DMA((T,)),
+            DMA((F,)), DMA((F,)), DMA((F,)), DMA((F,)), DMA((T,)), DMA((T,)),
+            DMA((3,)), DMA((3,)), DMA((3,)), DMA((3,)), DMA((3,)), DMA((4,)),
+        ],
+        compiler_params=pltpu.CompilerParams(
+            collective_id=0, has_side_effects=True, vmem_limit_bytes=63 * 2**20
+        ),
+        name="exchange",
+    )(saved_input.T, cot_forget.T, cot_value.T, *bases, *moments_in, *weights)
+
+    blocks = 3
+    deep = half // blocks
+    entries = float(width * cols * T)
+
+    def const(*shape):
+        return pl.BlockSpec(shape, lambda j, at: (0,) * len(shape))
+
+    def rows_of(count):
+        return pl.BlockSpec((deep, count), lambda j, at: (j, 0))
+
+    one_out = [
+        jax.ShapeDtypeStruct((ranks, cols), f32), jax.ShapeDtypeStruct((ranks, cols), f32),
+        jax.ShapeDtypeStruct((cols, rows), f32), jax.ShapeDtypeStruct((cols, rows), f32),
+        jax.ShapeDtypeStruct((cols, width), bf16),
+    ]
+    one_spec = [const(ranks, cols), const(ranks, cols), rows_of(rows), rows_of(rows), rows_of(width)]
+    results = pl.pallas_call(
+        functools.partial(finish, F, entries),
+        out_shape=one_out * 2,
+        grid_spec=pltpu.PrefetchScalarGridSpec(
+            num_scalar_prefetch=1,
+            grid=(2 * blocks,),
+            in_specs=[
+                const(2 * ranks, cols),
+                pl.BlockSpec((2, deep, rank), lambda j, at: (0, j, 0)),
+                const(T, 2, 8, LANES),
+                pl.BlockSpec((F, 1, tiles, deep, LANES), lambda j, at: (0, j // blocks, 0, j % blocks, 0)),
+                const(rank, width), const(rank, width), rows_of(rows), rows_of(rows),
+                *([const(ranks, cols)] * 4),
+            ],
+            out_specs=one_spec * 2,
+        ),
+        compiler_params=pltpu.CompilerParams(
+            dimension_semantics=("arbitrary",), vmem_limit_bytes=32 * 2**20
+        ),
+        name="finish",
+    )(lax.axis_index("fs").reshape(1), projected, direction, squares, gathered, *bases, *weights, *moments_in)
+    return tuple(r if i % 5 < 2 else r.T for i, r in enumerate(results))
+
+
+def program(F, T, *args):
+    tokens, cols = args[0].shape
+    ranks = args[5].shape[0]
+    rows = args[9].shape[0]
+    block_fits = tokens == T * LANES and cols % 96 == 0 and ranks % 8 == 0
+    rows_fit = rows > LANES and rows % LANES == LANES // 2
+    if F == 4 and T % 2 == 0 and block_fits and rows_fit:
+        return kernel_body(F, T, *args)
+    return body(*args)
+
+
 def solution(mesh):
-    in_specs = (
-        P("fs", "tp"),
-        P("fs", "tp"),
-        P("fs", "tp"),
-        P(),
-        P(),
-        P("fs", "tp"),
-        P("fs", "tp"),
-        P("fs", "tp"),
-        P("fs", "tp"),
-        P("fs", "tp"),
-        P("fs", "tp"),
-    )
-    out_specs = (
-        P("fs", "tp"),
-        P("fs", "tp"),
-        P("fs", "tp"),
-        P("fs", "tp"),
-        P(None, "tp"),
-        P("fs", "tp"),
-        P("fs", "tp"),
-        P("fs", "tp"),
-        P("fs", "tp"),
-        P(None, "tp"),
-    )
-    return jax.shard_map(body, mesh=mesh, in_specs=in_specs, out_specs=out_specs, check_vma=False)
+    split = P("fs", "tp")
+    in_specs = (split, split, split, P(), P()) + (split,) * 6
+    out_specs = (split, split, split, split, P(None, "tp")) * 2
+    inner = functools.partial(program, mesh.shape["fs"], mesh.shape["tp"])
+    return jax.shard_map(inner, mesh=mesh, in_specs=in_specs, out_specs=out_specs, check_vma=False)

time: 282 us -> 96.6 us (0.34)
  waiting for transfers between devices: 171 us -> 0 us
  Pallas kernels: 0 us -> 85.3 us
  blocking collectives: 66.8 us -> 0 us
  between operations: 16 us -> 0.72 us
  matrix products: 11.2 us -> 0 us
  other arithmetic: 6.67 us -> 0 us
    pallas_call x0 -> x2, Pallas kernels: none -> 85.3 us  [the longest x1 77 us: kernel_body(): pl.pallas_call(functools.partial(exchange, F, T), out_shape=(jax.ShapeDty...]
    psum x1 -> x0, waiting for transfers between devices: 66.5 us -> none  [body(): lax.psum((partial_forget, partial_value), 'tp')]
    all_gather x2 -> x0, waiting for transfers between devices: 64 us -> none  [the longest x1 32.4 us: body(): lax.all_gather(new_weight_forget.astype(jnp.bfloat16), 'fs', axis=0, tile...]
    unnamed x5 -> x0, waiting for transfers between devices: 40.9 us -> none
    psum x1 -> x0, blocking collectives: 39 us -> none  [body(): lax.psum((jnp.sum(update_forget * update_forget), jnp.sum(update_value *...]
    all_gather x2 -> x0, blocking collectives: 27.8 us -> none  [the longest x1 14.1 us: body(): lax.all_gather(direction_value, 'fs', axis=0, tiled=True)]
    dot_general x6 -> x0, matrix products: 11.2 us -> none  [the longest x2 3.49 us: contract(): lax.dot_general(left_part, right_part, (((0,), (0,)), ((), ())), precisio...]
    unnamed x25 -> x24, local copies, waits for them, and re-layouts: 4.64 us -> 10.1 us
  transfers between devices with their start and end apart: 4 -> 0, of which waited for: 4 -> 0; matrix products, arithmetic and copies ran while one was open for 3% -> 0% of each run, Pallas kernels for 0% -> 0%
where the time goes in v1:
time: 96.6 us; the launch traced here: 96.2 us
  Pallas kernels  85.3 us (88%)
  local copies, waits for them, and re-layouts  10.1 us (10%)
    pallas_call x1, Pallas kernels, kernel_body(): pl.pallas_call(functools.partial(exchange, F, T), out_shape=(jax.ShapeDty...  77 us
    unnamed x24, local copies, waits for them, and re-layouts  10.1 us
    pallas_call x1, Pallas kernels, kernel_body(): pl.pallas_call(functools.partial(finish, F, entries), out_shape=one_out *...  8.3 us

profile of v1, /device:TPU:0, one launch (start us, length us, event | category | flops | bytes accessed | tf_op | source)
XLA Modules:
  0.0 96.2 jit_solution(11592139573752592840)
XLA Ops:
  0.6 0.0 copy-start.2
  0.7 0.0 copy-start.5
  0.7 0.0 copy-start.6
  0.7 77.0 %exchange.1 = (f32[144,288]{1,0:T(8,128)}, bf16[2,288,288]{2,1,0:T(8,128)(2,1)}, f32[8,2,8,128]{3,2,1,0:T(8,128)}, bf16[4,2,9,144,128]{4,3,2,1,0:T(8,128)(2,1)}) custom-call(bf16[288,1024]{1,0:T(8,128)(2,1)} %bitcast.22, bf16[288,1024]{1,0:T(8,128)(2,1)} %bitcast.23, bf16[288,1024]{1,0:T(8,128)(2,1)} %bitcast.24, bf16[288,2304]{1,0:T(8,128)(2,1)} %bitcast.14, ...), custom_call_target="tpu_custom_call" | custom-call | tf_op jit(solution)/shard_map/exchange/pallas_call | solution.py:397
  77.7 0.0 copy-done.2
  77.7 0.0 copy-done.5
  77.7 0.0 copy-done.6
  77.8 0.0 copy-start
  77.8 1.3 %copy-done = bf16[2304,288]{0,1:T(8,128)(2,1)S(1)} copy-done((bf16[2304,288]{0,1:T(8,128)(2,1)S(1)}, bf16[2304,288]{0,1:T(8,128)(2,1)}, u32[]{:S(2)}) %copy-start) | copy-done | bytes 1327128
  79.1 0.0 copy-start.1
  79.1 1.3 %copy-done.1 = bf16[2304,288]{0,1:T(8,128)(2,1)S(1)} copy-done((bf16[2304,288]{0,1:T(8,128)(2,1)S(1)}, bf16[2304,288]{0,1:T(8,128)(2,1)}, u32[]{:S(2)}) %copy-start.1) | copy-done | bytes 1327128
  80.4 0.0 copy-start.3
  80.4 1.1 %copy-done.3 = f32[576,288]{0,1:T(8,128)S(1)} copy-done((f32[576,288]{0,1:T(8,128)S(1)}, f32[576,288]{0,1:T(8,128)}, u32[]{:S(2)}) %copy-start.3) | copy-done | bytes 663576
  81.5 0.0 copy-start.4
  81.5 1.7 %copy-done.4 = bf16[4,2,9,144,128]{4,3,2,1,0:T(8,128)(2,1)S(1)} copy-done((bf16[4,2,9,144,128]{4,3,2,1,0:T(8,128)(2,1)S(1)}, bf16[4,2,9,144,128]{4,3,2,1,0:T(8,128)(2,1)}, u32[]{:S(2)}) %copy-start.4) | copy-done | bytes 2654232
  83.3 0.0 copy-start.7
  83.3 0.9 copy-done.7
  84.2 0.0 copy-start.8
  84.2 0.9 copy-done.8
  85.1 0.0 copy-start.9
  85.1 1.0 %copy-done.9 = bf16[2,288,288]{2,1,0:T(8,128)(2,1)S(1)} copy-done((bf16[2,288,288]{2,1,0:T(8,128)(2,1)S(1)}, bf16[2,288,288]{2,1,0:T(8,128)(2,1)}, u32[]{:S(2)}) %copy-start.9) | copy-done | bytes 331800
  86.1 0.9 copy-done.10
  87.0 0.8 copy-done.11
  87.9 8.3 %finish.1 = (f32[72,288]{1,0:T(8,128)}, f32[72,288]{1,0:T(8,128)}, f32[288,576]{1,0:T(8,128)}, f32[288,576]{1,0:T(8,128)}, bf16[288,2304]{1,0:T(8,128)(2,1)}, /*...) custom-call(s32[1]{0:T(128)} %bitcast.at_ref, ...), custom_call_target="tpu_custom_call" | custom-call | tf_op jit(solution)/shard_map/finish/pallas_call | solution.py:450
  (2 shorter events, 0.0 us)
Async XLA Ops:
  0.6 77.1 %copy-start.2 = (f32[576,288]{0,1:T(8,128)S(1)}, f32[576,288]{0,1:T(8,128)}, u32[]{:S(2)}) copy-start(f32[576,288]{0,1:T(8,128)} %param.20) | copy-start | bytes 1990660
  0.7 77.1 %copy-start.5 = (f32[72,288]{1,0:T(8,128)S(1)}, f32[72,288]{1,0:T(8,128)}, u32[]{:S(2)}) copy-start(f32[72,288]{1,0:T(8,128)} %ff.1) | copy-start | bytes 248836
  0.7 77.1 %copy-start.6 = (f32[72,288]{1,0:T(8,128)S(1)}, f32[72,288]{1,0:T(8,128)}, u32[]{:S(2)}) copy-start(f32[72,288]{1,0:T(8,128)} %fv.1) | copy-start | bytes 248836
  77.8 1.3 %copy-start = (bf16[2304,288]{0,1:T(8,128)(2,1)S(1)}, bf16[2304,288]{0,1:T(8,128)(2,1)}, u32[]{:S(2)}) copy-start(bf16[2304,288]{0,1:T(8,128)(2,1)} %param.14) | copy-start | bytes 3981316
  79.1 1.3 %copy-start.1 = (bf16[2304,288]{0,1:T(8,128)(2,1)S(1)}, bf16[2304,288]{0,1:T(8,128)(2,1)}, u32[]{:S(2)}) copy-start(bf16[2304,288]{0,1:T(8,128)(2,1)} %param.15) | copy-start | bytes 3981316
  80.4 1.1 %copy-start.3 = (f32[576,288]{0,1:T(8,128)S(1)}, f32[576,288]{0,1:T(8,128)}, u32[]{:S(2)}) copy-start(f32[576,288]{0,1:T(8,128)} %param.21) | copy-start | bytes 1990660
  81.5 1.7 %copy-start.4 = (bf16[4,2,9,144,128]{4,3,2,1,0:T(8,128)(2,1)S(1)}, bf16[4,2,9,144,128]{4,3,2,1,0:T(8,128)(2,1)}, u32[]{:S(2)}) copy-start(bf16[4,2,9,144,128]{4,3,2,1,0:T(8,128)(2,1)} %get-tuple-element.27.wg) | copy-start | bytes 7962628
  83.3 0.9 copy-start.7
  84.2 0.9 copy-start.8
  85.1 1.0 %copy-start.9 = (bf16[2,288,288]{2,1,0:T(8,128)(2,1)S(1)}, bf16[2,288,288]{2,1,0:T(8,128)(2,1)}, u32[]{:S(2)}) copy-start(bf16[2,288,288]{2,1,0:T(8,128)(2,1)} %get-tuple-element.25.d) | copy-start | bytes 995332
  86.1 0.9 copy-start.10
  87.0 0.8 copy-start.11

commit v2 on v1

--- a/solution.py
+++ b/solution.py
@@ -151,15 +151,12 @@
     pr_out, d_out, ss_out, wg_out,
     s, c, b, fm, sm, w, sg, z, zg, psend, prx, pr, dg, d, ss, wg,
     in_sem, sg_own, sg_send, sg_recv, z_send, z_recv, zf_send, zf_recv,
-    p_send, p_recv, d_send, d_recv, n_send, n_recv, w_send, w_recv, wl_send, wl_recv, out_sem, wo_sem,
+    p_send, p_recv, d_send, d_recv, n_send, n_recv, w_send, w_recv, out_sem, own_out, wo_sem,
 ):
     f = lax.axis_index("fs")
     t = lax.axis_index("tp")
     ranks = psend.shape[1] // 2
     block = zg.shape[3]
-    right = lax.rem(f + 1, F)
-    left = lax.rem(f + F - 1, F)
-    far = lax.rem(f + 2, F)
     pair = t + 1 - 2 * lax.rem(t, 2)
 
     def tp_at(k):
@@ -210,13 +207,49 @@
         copy = push(s.at[:, tokens(tp_at(k))], sg.at[t], sg_send.at[k], sg_recv.at[k], {"tp": tp_at(k)})
         copy.start()
         sends.append(copy)
-    own_right = [push(wg.at[f, p], wg.at[f, p], w_send.at[p], w_recv.at[p], {"fs": right}) for p in range(2)]
-    own_left = [push(wg.at[f, p], wg.at[f, p], wl_send.at[p], wl_recv.at[p], {"fs": left}) for p in range(2)]
-    own_right[0].start()
-    own_left[1].start()
-    own_right[1].start()
-    own_left[0].start()
-    sends += own_right + own_left
+    def travel(k, half, way):
+        block = fs_at(-k) if way == 0 else fs_at(k)
+        return push(
+            wg.at[block, half], wg.at[block, half],
+            w_send.at[way, k, half], w_recv.at[way, k, half], {"fs": fs_at(1 if way == 0 else -1)},
+        )
+
+    def passes_on(k, way):
+        place = f if way == 0 else F - 1 - f
+        return jnp.logical_and(place >= k, place < F - 1)
+
+    def comes_in(k, way):
+        place = f if way == 0 else F - 1 - f
+        return place >= k
+
+    def leave(k, half, way):
+        block = fs_at(-k) if way == 0 else fs_at(k)
+        return pltpu.make_async_copy(wg.at[block, half], wg_out.at[block, half], wo_sem.at[way, k - 1, half])
+
+    def relay(k, half):
+        for way in range(2):
+            @pl.when(comes_in(k, way))
+            def _():
+                block = fs_at(-k) if way == 0 else fs_at(k)
+                push(
+                    wg.at[f, half], wg.at[block, half],
+                    w_send.at[way, k - 1, half], w_recv.at[way, k - 1, half],
+                    {"fs": fs_at(-1 if way == 0 else 1)},
+                ).wait_recv()
+
+                if k < F - 1:
+                    @pl.when(passes_on(k, way))
+                    def _():
+                        travel(k, half, way).start()
+
+                leave(k, half, way).start()
+
+    for half in range(2):
+        for way in range(2):
+            @pl.when(passes_on(0, way))
+            def _():
+                travel(0, half, way).start()
+    outs = [fetch(wg.at[f], wg_out.at[f], own_out)]
 
     load_own.wait()
     for copy in load_b:
@@ -236,6 +269,7 @@
         sends.append(copy)
     to_pair.start()
     sends.append(to_pair)
+    relay(1, 0)
 
     for copy in load_c:
         copy.wait()
@@ -256,6 +290,8 @@
         copy.start()
         sends.append(copy)
         partial = add(partial, source)
+        if k == chips - 1:
+            relay(1, 1)
     for k in range(1, chips):
         source = lax.rem(pair - 2 * k + T, T)
         push(z, zg.at[source], zf_send.at[k], zf_recv.at[k], {"tp": pair}).wait_recv()
@@ -271,14 +307,7 @@
         copy.start()
         sends.append(copy)
 
-    push(wg.at[f, 0], wg.at[left, 0], w_send.at[0], w_recv.at[0], {"fs": left}).wait_recv()
-    on_right = push(wg.at[left, 0], wg.at[left, 0], w_send.at[2], w_recv.at[2], {"fs": right})
-    on_right.start()
-    push(wg.at[f, 1], wg.at[right, 1], wl_send.at[1], wl_recv.at[1], {"fs": right}).wait_recv()
-    on_left = push(wg.at[right, 1], wg.at[right, 1], wl_send.at[2], wl_recv.at[2], {"fs": left})
-    on_left.start()
-    sends += [on_right, on_left]
-
+    relay(2, 0)
     for copy in load_m:
         copy.wait()
     for k in (1, F - 1, *range(2, F - 1)):
@@ -288,11 +317,12 @@
     pr[...] = total
     new_first, new_second = new_moments(total, fm[...].reshape(total.shape), sm[...].reshape(total.shape))
     dg[f] = (new_first / jnp.sqrt(new_second)).astype(jnp.bfloat16)
-    outs = [fetch(pr, pr_out, out_sem.at[0])]
+    outs.append(fetch(pr, pr_out, out_sem.at[0]))
     for k in (1, F - 1, *range(2, F - 1)):
         copy = push(dg.at[f], dg.at[f], d_send.at[k], d_recv.at[k], {"fs": fs_at(k)})
         copy.start()
         sends.append(copy)
+    relay(2, 1)
     for k in (1, F - 1, *range(2, F - 1)):
         push(dg.at[f], dg.at[fs_at(-k)], d_send.at[k], d_recv.at[k], {"fs": fs_at(-k)}).wait_recv()
     gathered = dg[...].astype(jnp.float32)
@@ -317,14 +347,19 @@
         push(ss.at[t], ss.at[tp_at(-k)], n_send.at[k], n_recv.at[k], {"tp": tp_at(-k)}).wait_recv()
     outs.append(fetch(ss, ss_out, out_sem.at[2]))
 
-    outs.append(fetch(wg.at[f], wg_out.at[f], wo_sem.at[0]))
-    push(wg.at[f, 1], wg.at[left, 1], w_send.at[1], w_recv.at[1], {"fs": left}).wait_recv()
-    outs.append(fetch(wg.at[left], wg_out.at[left], wo_sem.at[1]))
-    push(wg.at[f, 0], wg.at[right, 0], wl_send.at[0], wl_recv.at[0], {"fs": right}).wait_recv()
-    outs.append(fetch(wg.at[right], wg_out.at[right], wo_sem.at[2]))
-    push(wg.at[left, 0], wg.at[far, 0], w_send.at[2], w_recv.at[2], {"fs": left}).wait_recv()
-    push(wg.at[right, 1], wg.at[far, 1], wl_send.at[2], wl_recv.at[2], {"fs": right}).wait_recv()
-    outs.append(fetch(wg.at[far], wg_out.at[far], wo_sem.at[3]))
+    for k in range(3, F):
+        for half in range(2):
+            relay(k, half)
+    for half in range(2):
+        for way in range(2):
+            for k in range(F - 1):
+                @pl.when(passes_on(k, way))
+                def _():
+                    travel(k, half, way).wait_send()
+            for k in range(1, F):
+                @pl.when(comes_in(k, way))
+                def _():
+                    leave(k, half, way).wait()
     for copy in outs:
         copy.wait()
     for copy in sends:
@@ -423,7 +458,7 @@
             VMEM((F, 2, tiles, half, LANES), bf16),
             DMA((11,)), DMA, DMA((T,)), DMA((T,)), DMA((T,)), DMA((T,)), DMA((T,)), DMA((T,)),
             DMA((F,)), DMA((F,)), DMA((F,)), DMA((F,)), DMA((T,)), DMA((T,)),
-            DMA((3,)), DMA((3,)), DMA((3,)), DMA((3,)), DMA((3,)), DMA((4,)),
+            DMA((2, F - 1, 2)), DMA((2, F - 1, 2)), DMA((3,)), DMA, DMA((2, F - 1, 2)),
         ],
         compiler_params=pltpu.CompilerParams(
             collective_id=0, has_side_effects=True, vmem_limit_bytes=63 * 2**20
@@ -464,7 +499,7 @@
             out_specs=one_spec * 2,
         ),
         compiler_params=pltpu.CompilerParams(
-            dimension_semantics=("arbitrary",), vmem_limit_bytes=32 * 2**20
+            dimension_semantics=("arbitrary",), vmem_limit_bytes=63 * 2**20
         ),
         name="finish",
     )(lax.axis_index("fs").reshape(1), projected, direction, squares, gathered, *bases, *weights, *moments_in)

time: 96.6 us -> 76.9 us (0.80)
  local copies, waits for them, and re-layouts: 10.1 us -> 0 us
  Pallas kernels: 85.3 us -> 76 us
    pallas_call x1, Pallas kernels: 77 us -> 65.3 us  [kernel_body(): pl.pallas_call(functools.partial(exchange, F, T), out_shape=(jax.ShapeDty...]
    unnamed x24 -> x0, local copies, waits for them, and re-layouts: 10.1 us -> none
    pallas_call x1, Pallas kernels: 8.3 us -> 10.7 us  [kernel_body(): pl.pallas_call(functools.partial(finish, F, entries), out_shape=one_out *...]
where the time goes in v2:
time: 76.9 us; the launch traced here: 76.6 us
  Pallas kernels  76 us (99%)
    pallas_call x1, Pallas kernels, kernel_body(): pl.pallas_call(functools.partial(exchange, F, T), out_shape=(jax.ShapeDty...  65.3 us
    pallas_call x1, Pallas kernels, kernel_body(): pl.pallas_call(functools.partial(finish, F, entries), out_shape=one_out *...  10.7 us

profile of v2, /device:TPU:0, one launch (start us, length us, event | category | flops | bytes accessed | tf_op | source)
XLA Modules:
  0.0 76.6 jit_solution(5507323154412252410)
XLA Ops:
  0.6 65.3 %exchange.1 = (f32[144,288]{1,0:T(8,128)}, bf16[2,288,288]{2,1,0:T(8,128)(2,1)}, f32[8,2,8,128]{3,2,1,0:T(8,128)}, bf16[4,2,9,144,128]{4,3,2,1,0:T(8,128)(2,1)}) custom-call(bf16[288,1024]{1,0:T(8,128)(2,1)} %bitcast.22, bf16[288,1024]{1,0:T(8,128)(2,1)} %bitcast.23, bf16[288,1024]{1,0:T(8,128)(2,1)} %bitcast.24, bf16[288,2304]{1,0:T(8,128)(2,1)} %bitcast.14, ...), custom_call_target="tpu_custom_call" | custom-call | tf_op jit(solution)/shard_map/exchange/pallas_call | solution.py:432
  66.0 10.7 %finish.1 = (f32[72,288]{1,0:T(8,128)}, f32[72,288]{1,0:T(8,128)}, f32[288,576]{1,0:T(8,128)}, f32[288,576]{1,0:T(8,128)}, bf16[288,2304]{1,0:T(8,128)(2,1)}, /*...) custom-call(s32[1]{0:T(128)} %bitcast.at_ref, ...), custom_call_target="tpu_custom_call" | custom-call | tf_op jit(solution)/shard_map/finish/pallas_call | solution.py:485
